TPU v7x, 32 devices: a whole 2x2x4 slice. The times are simulated.
32 devices in a mesh: dp: 4 (over y, x), kv: 4 (over z), tp: 2 (over core).
Axes of the slice: x: 2, y: 2, z: 4, core: 2. Of those that a mesh axis runs over, the one named last changes fastest.
Arguments:
- tokens: bfloat16 [8192, 2048], P(('dp', 'kv')), parts along dimension 0, may hold values from -60 to 60, as said below
- chosen: int32 [128, 16], P(('dp', 'kv')), parts along dimension 0, may hold values from -1 to 31, as said below
- query_weight: bfloat16 [2048, 1024], P('kv', 'tp'), may hold values from -0.125 to 0.125
- key_matrix: bfloat16 [2048, 128], P('kv', 'tp'), may hold values from -0.125 to 0.125
- value_matrix: bfloat16 [2048, 128], P('kv', 'tp'), may hold values from -0.125 to 0.125
- out_weight: bfloat16 [1024, 2048], P('tp', 'kv'), may hold values from -0.1875 to 0.1875
- out_gain: float32 [2048], replicated, may hold values from 0.1 to 1.9
Outputs:
- mixed_out: bfloat16 [8192, 2048], P(('dp', 'kv', 'tp')), parts along dimension 0
There are 4 independent parts, one for each index of `dp`. A program takes and returns all parts, laid end to end along the dimension named above; an argument that names none is the same for every part. Nothing has to cross between parts.
Inputs may be any that keep to these rules, and one draw needn't show every extreme that they name: tokens are of order one apart from few rows. chosen[g, 0] = g; every other entry of row g is -1 or a block below g, and the entries of a row other than -1 are distinct; the blocks that the rows of one device name on any single other device are at most 2 different ones, and this is reached.
All inputs are finite; a program needn't handle non-finite values.
Results may differ from a plain program's by a relative error of at most 0.012.
The roundings to bfloat16 on the way count: a program that leaves them out, or rounds other values in their place, can miss the bound.
Values may be sent and summed in bfloat16 or wider, within the bound.
A program may use at most 64 MiB of HBM per device.

v0:
```python
import jax
import jax.numpy as jnp
from jax import lax
from jax.sharding import PartitionSpec as P

HEAD_WIDTH = 64
BLOCK_LENGTH = 64


def per_device(tokens, chosen, query_weight, key_matrix, value_matrix, out_weight, out_gain):
    tok_rows = tokens.shape[0]
    blocks = tok_rows // BLOCK_LENGTH
    device = lax.axis_index("kv")
    kv_count = lax.axis_size("kv")
    whole_query, whole_key, whole_value = (
        lax.all_gather(query_weight, "kv", axis=0, tiled=True),
        lax.all_gather(key_matrix, "kv", axis=0, tiled=True),
        lax.all_gather(value_matrix, "kv", axis=0, tiled=True),
    )
    query_rows = jnp.dot(tokens, whole_query, preferred_element_type=jnp.float32).astype(
        jnp.bfloat16
    )
    key_rows = jnp.dot(tokens, whole_key, preferred_element_type=jnp.float32).astype(jnp.bfloat16)
    value_rows = jnp.dot(tokens, whole_value, preferred_element_type=jnp.float32).astype(
        jnp.bfloat16
    )
    paired = jnp.concatenate([key_rows, value_rows], axis=1)
    pair_width = paired.shape[1]
    safe_ids = jnp.maximum(chosen, 0)
    everyone = lax.all_gather(paired, "kv", axis=0, tiled=True).reshape(
        kv_count * blocks, BLOCK_LENGTH, pair_width
    )
    picked = jnp.take(everyone, safe_ids, axis=0)
    head_count = query_rows.shape[1] // HEAD_WIDTH
    grouped = query_rows.reshape(blocks, BLOCK_LENGTH, head_count, HEAD_WIDTH)
    offsets = jnp.arange(BLOCK_LENGTH, dtype=jnp.int32)
    query_pos = (device * blocks + jnp.arange(blocks, dtype=jnp.int32))[
        :, None
    ] * BLOCK_LENGTH + offsets[None, :]
    key_pos = safe_ids[:, :, None] * BLOCK_LENGTH + offsets[None, None, :]
    visible = (chosen >= 0)[:, None, :, None] & (
        key_pos[:, None, :, :] <= query_pos[:, :, None, None]
    )

    def attend_block(inputs):
        query_block, pair_block, seen = inputs
        block_keys = pair_block[..., :HEAD_WIDTH]
        block_values = pair_block[..., HEAD_WIDTH:]
        scores = jnp.einsum(
            "qgd,skd->gqsk", query_block, block_keys, preferred_element_type=jnp.float32
        ) * HEAD_WIDTH ** (-0.5)
        scores = jnp.where(seen[None], scores, -1e30)
        row_max = jnp.max(scores, axis=(2, 3), keepdims=True)
        expon = jnp.exp(scores - row_max)
        row_sum = jnp.sum(expon, axis=(2, 3), keepdims=True)
        weights_bf = (expon / row_sum).astype(jnp.bfloat16)
        result = jnp.einsum(
            "gqsk,skd->qgd", weights_bf, block_values, preferred_element_type=jnp.float32
        )
        return result.astype(jnp.bfloat16)

    attended = lax.map(attend_block, (grouped, picked, visible))
    attended = attended.reshape(tok_rows, head_count * HEAD_WIDTH)
    whole_out = lax.all_gather(out_weight, "kv", axis=1, tiled=True)
    mixed = lax.psum_scatter(
        jnp.dot(attended, whole_out, preferred_element_type=jnp.float32).astype(jnp.bfloat16),
        "tp",
        scatter_dimension=0,
        tiled=True,
    ).astype(jnp.float32)
    normed = mixed * lax.rsqrt(jnp.mean(mixed * mixed, axis=-1, keepdims=True) + 1e-06) * out_gain
    return normed.astype(jnp.bfloat16)


def solution(mesh):
    placed = (
        P(("dp", "kv"), None),
        P(("dp", "kv"), None),
        P("kv", "tp"),
        P("kv", "tp"),
        P("kv", "tp"),
        P("tp", "kv"),
        P(),
    )
    return jax.shard_map(
        per_device,
        mesh=mesh,
        in_specs=placed,
        out_specs=P(("dp", "kv", "tp"), None),
        check_vma=False,
    )
```

profile of v0, /device:TPU:0, one launch (start us, length us, event | category | flops | bytes accessed | tf_op | source)
XLA Modules:
  0.0 154.0 jit_solution(18030068477290165004)
XLA Ops:
  9.5 16.8 %all_gather.16 = bf16[2048,64]{0,1:T(8,128)(2,1)S(1)} all-gather(bf16[512,64]{0,1:T(8,128)(2,1)} %param.13), channel_id=1, replica_groups=mesh['dp'=4,'kv'=4,'tp'=2] {'kv'}, dimensions={0}, use_global_device_ids=true | all-gather | bytes 327680 | tf_op jit(solution)/shard_map/all_gather | solution.py:18
  26.4 17.1 %all_gather.15 = bf16[2048,64]{0,1:T(8,128)(2,1)S(1)} all-gather(bf16[512,64]{0,1:T(8,128)(2,1)} %param.12), channel_id=1, replica_groups=mesh['dp'=4,'kv'=4,'tp'=2] {'kv'}, dimensions={0}, use_global_device_ids=true | all-gather | bytes 327680 | tf_op jit(solution)/shard_map/all_gather | solution.py:17
  45.1 22.0 %all_gather.17 = bf16[2048,128]{0,1:T(8,128)(2,1)S(1)} all-gather(bf16[512,128]{0,1:T(8,128)(2,1)S(1)} %pad_maximum_fusion), channel_id=1, replica_groups=mesh['dp'=4,'kv'=4,'tp'=2] {'kv'}, dimensions={0}, use_global_device_ids=true | all-gather | bytes 655360 | tf_op jit(solution)/shard_map/all_gather | solution.py:30
  67.6 2.2 %gather_fusion = bf16[128,64,128]{2,1,0:T(8,128)(2,1)} fusion(bf16[32,64,128]{2,1,0:T(8,128)(2,1)S(1)} %bitcast.82, s32[1024]{0:T(1024)S(1)} %pad_clamp_fusion), kind=kCustom, calls=%fused_computation | custom fusion | bytes 4194816 | tf_op jit(solution)/shard_map/jit(_take)/gather | solution.py:33
  69.7 3.2 %broadcast_select_fusion = bf16[8,16,64,128]{3,2,1,0:T(8,128)(2,1)} fusion(bf16[8,16,64,128]{3,2,1,0:T(8,128)(2,1)} %bitcast.83, pred[8,16]{1,0:T(8,128)(4,1)S(1)} %get-tuple-element.56), kind=kLoop, calls=%fused_computation.27 | loop fusion | flops 1048576 | bytes 4194432 | tf_op jit(solution)/shard_map/jit(_take)/select_n | solution.py:33
  72.9 1.5 compare_and_fusion
  74.5 3.6 %convolution_convert_fusion.1 = bf16[512,512]{1,0:T(8,128)(2,1)} fusion(bf16[512,2048]{1,0:T(8,128)(2,1)S(1)} %copy-done, bf16[2048,512]{1,0:T(8,128)(2,1)} %all-gather.3.cloned.1.call-done), kind=kOutput, calls=%fused_computation.28 | convolution fusion | flops 1074003968 | bytes 4718592 | tf_op jit(solution)/shard_map/dot_general | solution.py:20
  78.1 2.4 %reshape.58 = bf16[8,64,8,64]{3,2,1,0:T(8,128)(2,1)} reshape(bf16[512,512]{1,0:T(8,128)(2,1)} %convolution_convert_fusion.1) | data formatting | bytes 1048576 | tf_op jit(solution)/shard_map/reshape | solution.py:35
  80.5 47.3 %while.10 = (s32[]{:T(128)}, bf16[8,64,8,64]{3,2,1,0:T(8,128)(2,1)}, bf16[8,16,64,128]{3,2,1,0:T(8,128)(2,1)}, pred[8,64,16,64]{1,3,2,0:T(8,128)(4,1)S(1)}, bf16[8,64,8,64]{3,2,1,0:T(8,128)(2,1)}, /*index=5*/s32[]{:T(128)}) while((s32[]{:T(128)}, bf16[8,64,8,64]{3,2,1,0:T(8,128)(2,1)}, bf16[8,16,64,128]{3,2,1,0:T(8,128)(2,1)}, ...), condition=%wide.region_3.4_spmd, body=%wide.region_0.3_spmd.sunk | while | flops 140540928 | bytes 8268369 | solution.py:62
  83.3 1.0 fusion.24
  84.3 1.2 fusion.25
  90.2 1.2 fusion.25
  96.2 1.2 fusion.25
  102.1 1.2 fusion.25
  108.0 1.2 fusion.25
  113.9 1.2 fusion.25
  119.8 1.2 fusion.25
  124.7 1.0 fusion.24
  125.7 1.2 fusion.25
  127.8 1.9 %reshape.59 = bf16[512,512]{1,0:T(8,128)(2,1)S(1)} reshape(bf16[8,64,8,64]{3,2,1,0:T(8,128)(2,1)} %get-tuple-element.32) | data formatting | bytes 1048576 | tf_op jit(solution)/shard_map/reshape | solution.py:63
  129.7 4.2 %convolution_convert_fusion = bf16[512,2048]{1,0:T(8,128)(2,1)} fusion(bf16[512,512]{1,0:T(8,128)(2,1)S(1)} %reshape.59, bf16[512,2048]{1,0:T(8,128)(2,1)} %all-gather.5.cloned.1.call-done), kind=kOutput, calls=%fused_computation.21 | convolution fusion | flops 1074790400 | bytes 4718592 | tf_op jit(solution)/shard_map/dot_general | solution.py:66
  133.9 9.6 %reduce-scatter.2.cloned.1.call-done = bf16[256,2048]{1,0:T(8,128)(2,1)} async-done(((bf16[512,2048]{1,0:T(8,128)(2,1)}), bf16[256,2048]{1,0:T(8,128)(2,1)}) %reduce-scatter.2.cloned.1.call-update) | async-done | bytes 1048592 | tf_op jit(solution)/shard_map/reduce_scatter | solution.py:65
  143.5 1.5 fusion.9
  145.0 2.5 %fusion.11 = bf16[256,2048]{1,0:T(8,128)(2,1)} fusion(bf16[256,2048]{1,0:T(8,128)(2,1)} %reduce-scatter.2.cloned.1.call-done, f32[2048]{0:T(1024)S(1)} %copy-done.1, f32[256]{0:T(256)S(1)} %add_rsqrt_fusion), kind=kLoop, calls=%fused_computation.26 | loop fusion | flops 2097152 | bytes 2106368 | tf_op jit(solution)/shard_map/convert_element_type | solution.py:72
  (79 shorter events, 40.0 us)
Async XLA Ops:
  6.5 37.0 %copy-start = (bf16[512,2048]{1,0:T(8,128)(2,1)S(1)}, bf16[512,2048]{1,0:T(8,128)(2,1)}, u32[]{:S(2)}) copy-start(bf16[512,2048]{1,0:T(8,128)(2,1)} %param.9) | copy-start | bytes 6291460
  6.5 67.9 %all-gather.3.cloned.1.call-start = ((), (), s32[]{:S(2)}) async-start(), calls=%async_computation.1 | async-start | bytes 2621440 | tf_op jit(solution)/shard_map/all_gather | solution.py:16
  7.3 122.4 %all-gather.5.cloned.1.call-start = ((), (), s32[]{:S(2)}) async-start(), calls=%async_computation.2 | async-start | bytes 2621440 | tf_op jit(solution)/shard_map/all_gather | solution.py:64
  8.0 135.5 %reduce-scatter.2.cloned.1.call-start = ((), (), s32[]{:S(2)}) async-start(), calls=%async_computation.3 | async-start | bytes 3145728 | tf_op jit(solution)/shard_map/reduce_scatter | solution.py:65
  133.8 11.2 %copy-start.1 = (f32[2048]{0:T(1024)S(1)}, f32[2048]{0:T(1024)}, u32[]{:S(2)}) copy-start(f32[2048]{0:T(1024)} %param.15) | copy-start | bytes 24580
Sparse Core Ops, SparseCore 0:
  8.9 61.9 all-gather.2
  72.5 44.4 all-gather.4
  134.0 9.4 reduce-scatter.1
where the time goes:
time: 155 us; the launch traced here: 154 us
  blocking collectives  56 us (36%)
  local copies, waits for them, and re-layouts  28.5 us (18%)
  matrix products  26.5 us (17%)
  other arithmetic  18.5 us (12%)
  between operations  13.2 us (9%)
  waiting for transfers between devices  11.1 us (7%)
    all_gather x1, blocking collectives, per_device(): lax.all_gather(paired, 'kv', axis=0, tiled=True)  22 us
    all_gather x1, blocking collectives, per_device(): lax.all_gather(key_matrix, 'kv', axis=0, tiled=True)  17.1 us
    all_gather x1, blocking collectives, per_device(): lax.all_gather(value_matrix, 'kv', axis=0, tiled=True)  16.8 us
    dot_general x8, matrix products, attend_block(): jnp.einsum('gqsk,skd->qgd', weights_bf, block_values, preferred_element_t...  9.99 us
    reduce_scatter x1, waiting for transfers between devices, per_device(): lax.psum_scatter(jnp.dot(attended, whole_out, preferred_element_type=jnp....  9.61 us
    reduce_sum x8, other arithmetic, attend_block(): row_sum = jnp.sum(expon, axis=(2, 3), keepdims=True)  8.16 us
    squeeze x8, local copies, waits for them, and re-layouts, per_device(): attended = lax.map(attend_block, (grouped, picked, visible))  7.8 us
    dynamic_slice x8, local copies, waits for them, and re-layouts, per_device(): attended = lax.map(attend_block, (grouped, picked, visible))  7.37 us
  transfers between devices with their start and end apart: 3, of which 1 were waited for; matrix products, arithmetic and copies ran while one was open for 42% of the time, Pallas kernels for 0%

commit v1 on v0

--- a/solution.py
+++ b/solution.py
@@ -2,9 +2,29 @@
 import jax.numpy as jnp
 from jax import lax
 from jax.sharding import PartitionSpec as P
+from jax.lax import axis_index, ppermute, psum
 
 HEAD_WIDTH = 64
 BLOCK_LENGTH = 64
+
+
+def reach_squares(body, chip_axis, d_out):
+    current_arr, big, moved = (
+        psum(1, axis_name=chip_axis),
+        axis_index(chip_axis),
+        body.shape[d_out],
+    )
+    shelf = [(to_i, (to_i + 1) % current_arr) for to_i in range(current_arr)]
+    x_now = jnp.zeros(
+        (*body.shape[:d_out], current_arr * moved, *body.shape[d_out + 1 :]), body.dtype
+    )
+    finding = body
+    for num in range(current_arr):
+        current_block = (big - num) % current_arr
+        x_now = lax.dynamic_update_slice_in_dim(x_now, finding, current_block * moved, axis=d_out)
+        if num < current_arr - 1:
+            finding = ppermute(finding, axis_name=chip_axis, perm=shelf)
+    return x_now
 
 
 def per_device(tokens, chosen, query_weight, key_matrix, value_matrix, out_weight, out_gain):
@@ -27,9 +47,7 @@
     paired = jnp.concatenate([key_rows, value_rows], axis=1)
     pair_width = paired.shape[1]
     safe_ids = jnp.maximum(chosen, 0)
-    everyone = lax.all_gather(paired, "kv", axis=0, tiled=True).reshape(
-        kv_count * blocks, BLOCK_LENGTH, pair_width
-    )
+    everyone = reach_squares(paired, "kv", 0).reshape(kv_count * blocks, BLOCK_LENGTH, pair_width)
     picked = jnp.take(everyone, safe_ids, axis=0)
     head_count = query_rows.shape[1] // HEAD_WIDTH
     grouped = query_rows.reshape(blocks, BLOCK_LENGTH, head_count, HEAD_WIDTH)

time: 155 us -> 158 us (1.019)
  waiting for transfers between devices: 11.1 us -> 34.3 us
  blocking collectives: 56 us -> 34.3 us
  starting transfers between devices: 0.08 us -> 1.93 us
    ppermute x0 -> x3, waiting for transfers between devices: none -> 24 us  [reach_squares(): finding = ppermute(finding, axis_name=chip_axis, perm=shelf)]
    all_gather x1 -> x0, blocking collectives: 22 us -> none  [per_device(): lax.all_gather(paired, 'kv', axis=0, tiled=True)]
    broadcast_in_dim x8, local copies, waits for them, and re-layouts: 0.08 us -> 7.31 us  [attend_block(): scores = jnp.where(seen[None], scores, -1e+30)]
    dynamic_slice x8, local copies, waits for them, and re-layouts: 7.37 us -> 0.14 us  [per_device(): attended = lax.map(attend_block, (grouped, picked, visible))]
    ppermute x0 -> x3, starting transfers between devices: none -> 1.85 us  [reach_squares(): finding = ppermute(finding, axis_name=chip_axis, perm=shelf)]
  transfers between devices with their start and end apart: 3 -> 6, of which waited for: 1 -> 4; matrix products, arithmetic and copies ran while one was open for 42% -> 41% of each run, Pallas kernels for 0% -> 0%
where the time goes in v1:
time: 158 us; the launch traced here: 157 us
  waiting for transfers between devices  34.3 us (22%)
  blocking collectives  34.3 us (22%)
  local copies, waits for them, and re-layouts  28.2 us (18%)
  matrix products  26.5 us (17%)
  other arithmetic  18.3 us (12%)
  between operations  13.4 us (8%)
  starting transfers between devices  1.93 us (1%)
    ppermute x3, waiting for transfers between devices, reach_squares(): finding = ppermute(finding, axis_name=chip_axis, perm=shelf)  24 us
    all_gather x1, blocking collectives, per_device(): lax.all_gather(key_matrix, 'kv', axis=0, tiled=True)  17.7 us
    all_gather x1, blocking collectives, per_device(): lax.all_gather(value_matrix, 'kv', axis=0, tiled=True)  16.7 us
    dot_general x8, matrix products, attend_block(): jnp.einsum('gqsk,skd->qgd', weights_bf, block_values, preferred_element_t...  9.99 us
    reduce_scatter x1, waiting for transfers between devices, per_device(): lax.psum_scatter(jnp.dot(attended, whole_out, preferred_element_type=jnp....  9.47 us
    reduce_sum x8, other arithmetic, attend_block(): row_sum = jnp.sum(expon, axis=(2, 3), keepdims=True)  8.16 us
    squeeze x8, local copies, waits for them, and re-layouts, per_device(): attended = lax.map(attend_block, (grouped, picked, visible))  7.81 us
    broadcast_in_dim x8, local copies, waits for them, and re-layouts, attend_block(): scores = jnp.where(seen[None], scores, -1e+30)  7.31 us
  transfers between devices with their start and end apart: 6, of which 4 were waited for; matrix products, arithmetic and copies ran while one was open for 41% of the time, Pallas kernels for 0%

profile of v1, /device:TPU:0, one launch (start us, length us, event | category | flops | bytes accessed | tf_op | source)
XLA Modules:
  0.0 157.1 jit_solution(17025253862587367967)
XLA Ops:
  7.3 16.7 %all_gather.13 = bf16[2048,64]{0,1:T(8,128)(2,1)S(1)} all-gather(bf16[512,64]{0,1:T(8,128)(2,1)} %param.13), channel_id=1, replica_groups=mesh['dp'=4,'kv'=4,'tp'=2] {'kv'}, dimensions={0}, use_global_device_ids=true | all-gather | bytes 327680 | tf_op jit(solution)/shard_map/all_gather | solution.py:38
  24.0 17.7 %all_gather.12 = bf16[2048,64]{0,1:T(8,128)(2,1)S(1)} all-gather(bf16[512,64]{0,1:T(8,128)(2,1)} %param.12), channel_id=1, replica_groups=mesh['dp'=4,'kv'=4,'tp'=2] {'kv'}, dimensions={0}, use_global_device_ids=true | all-gather | bytes 327680 | tf_op jit(solution)/shard_map/all_gather | solution.py:37
  43.2 1.6 %collective-permute-start = (bf16[512,128]{0,1:T(8,128)(2,1)S(1)}, bf16[512,128]{0,1:T(8,128)(2,1)S(1)}, u32[]{:S(2)}, u32[]{:S(2)}) collective-permute-start(bf16[512,128]{0,1:T(8,128)(2,1)S(1)} %pad_maximum_fusion), channel_id=1, source_target_pairs={{0,2},{2,4},{4,6},{6,0},{1,3},{3,5},{5,7},{7,1},{8,10},{10,12},{12... | collective-permute-start | bytes 393224 | tf_op jit(solution)/shard_map/ppermute | solution.py:26
  45.1 2.6 %compare_and_fusion = pred[8,64,16,64]{1,3,2,0:T(8,128)(4,1)} fusion(s32[8,64]{1,0:T(8,128)S(1)} %iota_add_fusion.1, s32[8,16,64]{2,1,0:T(8,128)S(1)} %iota_add_fusion, pred[8,16]{1,0:T(8,128)(4,1)S(1)} %get-tuple-element.55), kind=kLoop, calls=%fused_computation.20 | loop fusion | flops 1048576 | bytes 559232 | tf_op jit(solution)/shard_map/and | solution.py:59
  47.8 5.9 %collective-permute-done = bf16[512,128]{0,1:T(8,128)(2,1)S(1)} collective-permute-done((bf16[512,128]{0,1:T(8,128)(2,1)S(1)}, bf16[512,128]{0,1:T(8,128)(2,1)S(1)}, u32[]{:S(2)}, u32[]{:S(2)}) %collective-permute-start) | collective-permute-done | bytes 131104 | tf_op jit(solution)/shard_map/ppermute | solution.py:26
  54.4 11.5 %collective-permute-done.1 = bf16[512,128]{0,1:T(8,128)(2,1)S(1)} collective-permute-done((bf16[512,128]{0,1:T(8,128)(2,1)S(1)}, bf16[512,128]{0,1:T(8,128)(2,1)S(1)}, u32[]{:S(2)}, u32[]{:S(2)}) %collective-permute-start.1) | collective-permute-done | bytes 131104 | tf_op jit(solution)/shard_map/ppermute | solution.py:26
  66.1 6.6 %collective-permute-done.2 = bf16[512,128]{0,1:T(8,128)(2,1)S(1)} collective-permute-done((bf16[512,128]{0,1:T(8,128)(2,1)S(1)}, bf16[512,128]{0,1:T(8,128)(2,1)S(1)}, u32[]{:S(2)}, u32[]{:S(2)}) %collective-permute-start.2) | collective-permute-done | bytes 131104 | tf_op jit(solution)/shard_map/ppermute | solution.py:26
  72.9 2.2 %gather_fusion = bf16[128,64,128]{2,1,0:T(8,128)(2,1)} fusion(bf16[32,64,128]{2,1,0:T(8,128)(2,1)S(1)} %bitcast.82, s32[1024]{0:T(1024)S(1)} %pad_clamp_fusion), kind=kCustom, calls=%fused_computation | custom fusion | bytes 4194816 | tf_op jit(solution)/shard_map/jit(_take)/gather | solution.py:51
  75.0 3.3 %broadcast_select_fusion = bf16[8,16,64,128]{3,2,1,0:T(8,128)(2,1)} fusion(bf16[8,16,64,128]{3,2,1,0:T(8,128)(2,1)} %bitcast.83, pred[8,16]{1,0:T(8,128)(4,1)S(1)} %get-tuple-element.56), kind=kLoop, calls=%fused_computation.27 | loop fusion | flops 1048576 | bytes 4194432 | tf_op jit(solution)/shard_map/jit(_take)/select_n | solution.py:51
  78.3 3.7 %convolution_convert_fusion.1 = bf16[512,512]{1,0:T(8,128)(2,1)} fusion(bf16[512,2048]{1,0:T(8,128)(2,1)S(1)} %copy-done, bf16[2048,512]{1,0:T(8,128)(2,1)} %all-gather.3.cloned.1.call-done), kind=kOutput, calls=%fused_computation.28 | convolution fusion | flops 1074003968 | bytes 4718592 | tf_op jit(solution)/shard_map/dot_general | solution.py:40
  82.0 1.6 %reshape.58 = bf16[8,64,8,64]{3,2,1,0:T(8,128)(2,1)S(1)} reshape(bf16[512,512]{1,0:T(8,128)(2,1)} %convolution_convert_fusion.1) | data formatting | bytes 1048576 | tf_op jit(solution)/shard_map/reshape | solution.py:53
  83.6 47.3 %while.10 = (s32[]{:T(128)}, bf16[8,64,8,64]{3,2,1,0:T(8,128)(2,1)}, bf16[8,16,64,128]{3,2,1,0:T(8,128)(2,1)}, pred[8,64,16,64]{1,3,2,0:T(8,128)(4,1)}, bf16[8,64,8,64]{3,2,1,0:T(8,128)(2,1)S(1)}, /*index=5*/s32[]{:T(128)}) while((s32[]{:T(128)}, bf16[8,64,8,64]{3,2,1,0:T(8,128)(2,1)}, bf16[8,16,64,128]{3,2,1,0:T(8,128)(2,1)}, ...), condition=%wide.region_3.4_spmd, body=%wide.region_0.3_spmd.sunk | while | flops 140540928 | bytes 8268369 | solution.py:80
  87.5 1.2 fusion.25
  93.4 1.2 fusion.25
  99.3 1.2 fusion.25
  105.3 1.2 fusion.25
  111.2 1.3 fusion.25
  117.1 1.2 fusion.25
  123.0 1.2 fusion.25
  131.0 1.9 %reshape.59 = bf16[512,512]{1,0:T(8,128)(2,1)S(1)} reshape(bf16[8,64,8,64]{3,2,1,0:T(8,128)(2,1)} %get-tuple-element.32) | data formatting | bytes 1048576 | tf_op jit(solution)/shard_map/reshape | solution.py:81
  132.9 4.2 %convolution_convert_fusion = bf16[512,2048]{1,0:T(8,128)(2,1)} fusion(bf16[512,512]{1,0:T(8,128)(2,1)S(1)} %reshape.59, bf16[512,2048]{1,0:T(8,128)(2,1)} %all-gather.5.cloned.1.call-done), kind=kOutput, calls=%fused_computation.21 | convolution fusion | flops 1074790400 | bytes 4718592 | tf_op jit(solution)/shard_map/dot_general | solution.py:84
  137.1 9.5 %reduce-scatter.2.cloned.1.call-done = bf16[256,2048]{1,0:T(8,128)(2,1)} async-done(((bf16[512,2048]{1,0:T(8,128)(2,1)}), bf16[256,2048]{1,0:T(8,128)(2,1)}) %reduce-scatter.2.cloned.1.call-update) | async-done | bytes 1048592 | tf_op jit(solution)/shard_map/reduce_scatter | solution.py:83
  146.5 1.5 fusion.9
  148.1 2.5 %fusion.11 = bf16[256,2048]{1,0:T(8,128)(2,1)} fusion(bf16[256,2048]{1,0:T(8,128)(2,1)} %reduce-scatter.2.cloned.1.call-done, f32[2048]{0:T(1024)S(1)} %copy-done.2, f32[256]{0:T(256)S(1)} %add_rsqrt_fusion), kind=kLoop, calls=%fused_computation.26 | loop fusion | flops 2097152 | bytes 2106368 | tf_op jit(solution)/shard_map/convert_element_type | solution.py:90
  (94 shorter events, 41.9 us)
Async XLA Ops:
  6.5 35.1 %copy-start = (bf16[512,2048]{1,0:T(8,128)(2,1)S(1)}, bf16[512,2048]{1,0:T(8,128)(2,1)}, u32[]{:S(2)}) copy-start(bf16[512,2048]{1,0:T(8,128)(2,1)} %param.9) | copy-start | bytes 6291460
  6.5 71.8 %all-gather.3.cloned.1.call-start = ((), (), s32[]{:S(2)}) async-start(), calls=%async_computation.1 | async-start | bytes 2621440 | tf_op jit(solution)/shard_map/all_gather | solution.py:36
  7.3 125.6 %all-gather.5.cloned.1.call-start = ((), (), s32[]{:S(2)}) async-start(), calls=%async_computation.2 | async-start | bytes 2621440 | tf_op jit(solution)/shard_map/all_gather | solution.py:82
  42.4 2.4 %copy-start.1 = (s32[8,16]{1,0:T(8,128)S(1)}, s32[8,16]{1,0:T(8,128)}, u32[]{:S(2)}) copy-start(s32[8,16]{1,0:T(8,128)} %param.10) | copy-start | bytes 1540
  43.2 10.4 %collective-permute-start = (bf16[512,128]{0,1:T(8,128)(2,1)S(1)}, bf16[512,128]{0,1:T(8,128)(2,1)S(1)}, u32[]{:S(2)}, u32[]{:S(2)}) collective-permute-start(bf16[512,128]{0,1:T(8,128)(2,1)S(1)} %pad_maximum_fusion), channel_id=1, source_target_pairs={{0,2},{2,4},{4,6},{6,0},{1,3},{3,5},{5,7},{7,1},{8,10},{10,12},{12... | collective-permute-start | bytes 393224 | tf_op jit(solution)/shard_map/ppermute | solution.py:26
  44.8 101.7 %reduce-scatter.2.cloned.1.call-start = ((), (), s32[]{:S(2)}) async-start(), calls=%async_computation.3 | async-start | bytes 3145728 | tf_op jit(solution)/shard_map/reduce_scatter | solution.py:83
  53.6 12.3 %collective-permute-start.1 = (bf16[512,128]{0,1:T(8,128)(2,1)S(1)}, bf16[512,128]{0,1:T(8,128)(2,1)S(1)}, u32[]{:S(2)}, u32[]{:S(2)}) collective-permute-start(bf16[512,128]{0,1:T(8,128)(2,1)S(1)} %collective-permute-done), channel_id=1, source_target_pairs={{0,2},{2,4},{4,6},{6,0},{1,3},{3,5},{5,7},{7,1},{8,10},{10,12},{12... | collective-permute-start | bytes 393224 | tf_op jit(solution)/shard_map/ppermute | solution.py:26
  65.9 6.8 %collective-permute-start.2 = (bf16[512,128]{0,1:T(8,128)(2,1)S(1)}, bf16[512,128]{0,1:T(8,128)(2,1)S(1)}, u32[]{:S(2)}, u32[]{:S(2)}) collective-permute-start(bf16[512,128]{0,1:T(8,128)(2,1)S(1)} %collective-permute-done.1), channel_id=1, source_target_pairs={{0,2},{2,4},{4,6},{6,0},{1,3},{3,5},{5,7},{7,1},{8,10},{10,12},{12... | collective-permute-start | bytes 393224 | tf_op jit(solution)/shard_map/ppermute | solution.py:26
  137.1 11.0 %copy-start.2 = (f32[2048]{0:T(1024)S(1)}, f32[2048]{0:T(1024)}, u32[]{:S(2)}) copy-start(f32[2048]{0:T(1024)} %param.15) | copy-start | bytes 24580
Sparse Core Ops, SparseCore 0:
  8.9 59.7 all-gather.2
  70.3 44.3 all-gather.4
  137.2 9.2 reduce-scatter.1
